TPU v7x, 256 devices: a whole 4x4x8 slice. The times are simulated.
256 devices in a mesh: ep: 64 (over z, x, core), tp: 4 (over y).
Axes of the slice: x: 4, y: 4, z: 8, core: 2. Of those that a mesh axis runs over, the one named last changes fastest.
Arguments:
- mixer_input: bfloat16 [32768, 2048], P('ep'), may hold values from -6 to 6
- mixer_gain: float32 [2048], replicated, may hold values from 0.1 to 1.9
- query_weight: bfloat16 [2048, 1024], P(None, 'tp'), may hold values from -0.125 to 0.125
- key_weight: bfloat16 [2048, 1024], P(None, 'tp'), may hold values from -0.125 to 0.125
- value_weight: bfloat16 [2048, 1024], P(None, 'tp'), may hold values from -0.125 to 0.125
- gate_weight: bfloat16 [2048, 1024], P(None, 'tp'), may hold values from -0.125 to 0.125
- head_gain: float32 [1024], P('tp'), may hold values from 0.1 to 1.9
- output_weight: bfloat16 [1024, 2048], P('tp'), may hold values from -0.1875 to 0.1875
- log_decay: float32 [32768, 8], P('ep', 'tp'), may hold values from -1 to 0, as said below
- expert_input: bfloat16 [32768, 2048], P(('ep', 'tp')), may hold values from -6 to 6
- expert_gain: float32 [2048], replicated, may hold values from 0.1 to 1.9
- routes: int32 [32768, 2], P(('ep', 'tp')), may hold values from 0 to 63, all different within a row; in each aligned block of 128 rows (0 to 127, 128 to 255, ...) at most 6 rows name the same one
- route_weight: float32 [32768, 2], P(('ep', 'tp')), may hold values from 0.1 to 1
- expert_gate: bfloat16 [64, 2048, 1024], P('ep', None, 'tp'), may hold values from -0.125 to 0.125
- expert_up: bfloat16 [64, 2048, 1024], P('ep', None, 'tp'), may hold values from -0.125 to 0.125
- expert_down: bfloat16 [64, 1024, 2048], P('ep', 'tp'), may hold values from -0.1875 to 0.1875
Outputs:
- mixer_output: bfloat16 [32768, 2048], P(('ep', 'tp'))
- expert_output: bfloat16 [32768, 2048], P(('ep', 'tp'))
Inputs may be any that keep to these rules, and one draw needn't show every extreme that they name: `routes`: each row names 2 different experts. Among the rows of one device no expert is named more than 6 times, and in every draw the rows of some device name some expert exactly 6 times. `log_decay`: negative values.
All inputs are finite; a program needn't handle non-finite values.
Results may differ from a plain program's by a relative error of at most 0.025.
Values may be sent and summed in bfloat16 or wider, within the bound.
A program may use at most 128 MiB of HBM per device.

v0:
```python
import jax
import jax.numpy as jnp
from jax import lax
from jax.sharding import Mesh
from jax.sharding import PartitionSpec as P

BLOCK = 128
EP = ("ep_0", "ep_1", "ep_2")
EP_TP = ("ep_0", "ep_1", "ep_2", "tp")
EPS = 1e-06


def filled_with(x, identity):
    return jax.tree.map(
        lambda part, zero: jnp.zeros_like(part) + jnp.asarray(zero, part.dtype), x, identity
    )


def carried_in(x, axes, combine, identity):
    before = start = filled_with(x, identity)
    running = x
    for axis in reversed(axes):
        peers, position = (lax.axis_size(axis), lax.axis_index(axis))
        pieces = jax.tree.map(
            lambda part, kind: lax.all_gather(part.astype(kind), axis),
            running,
            (jnp.bfloat16, jnp.bfloat16),
        )
        inside, running = (start, start)
        for k in range(peers):
            passed = k < position
            running = combine(
                running, jax.tree.map(lambda part, own: part[k].astype(own.dtype), pieces, x)
            )
            inside = jax.tree.map(lambda new, old: jnp.where(passed, new, old), running, inside)
        before = combine(inside, before)
    return before


def norm_rows(values, gain):
    floats = values.astype(jnp.float32)
    scale = lax.rsqrt(jnp.mean(floats * floats, axis=-1, keepdims=True) + EPS)
    return (floats * scale * gain).astype(jnp.bfloat16)


def rotate(values, position):
    half_dim = values.shape[-1] // 2
    frequency = 10000.0 ** (-jnp.arange(half_dim, dtype=jnp.float32) / half_dim)
    angles = position.astype(jnp.float32)[:, None] * frequency[None, :]
    cosine = jnp.cos(angles)[:, None, :]
    sine_part = jnp.sin(angles)[:, None, :]
    first_half = values[..., :half_dim]
    second = values[..., half_dim:]
    return jnp.concatenate(
        [first_half * cosine - second * sine_part, first_half * sine_part + second * cosine],
        axis=-1,
    )


def chain_pair(earlier, following):
    return (earlier[0] * following[0], following[0][:, None, None] * earlier[1] + following[1])


def mixer_half(
    mixer_input,
    mixer_gain,
    query_weight,
    key_weight,
    value_weight,
    gate_weight,
    head_gain,
    output_weight,
    log_decay,
):
    row_count = mixer_input.shape[0]
    head_count = log_decay.shape[1]
    mix_width = query_weight.shape[1]
    head_dim = mix_width // head_count
    normed = norm_rows(mixer_input, mixer_gain)

    def project(weight):
        return jnp.dot(normed, weight, preferred_element_type=jnp.float32).astype(jnp.bfloat16)

    queries = project(query_weight)
    keys_raw = project(key_weight)
    values_new = project(value_weight)
    gate_raw = project(gate_weight)
    position = lax.axis_index(EP) * row_count + jnp.arange(row_count, dtype=jnp.int32)
    q_rot = rotate(
        queries.astype(jnp.float32).reshape(row_count, head_count, head_dim), position
    ).astype(jnp.bfloat16)
    k_rot = (
        rotate(keys_raw.astype(jnp.float32).reshape(row_count, head_count, head_dim), position)
        * head_dim ** (-0.5)
    ).astype(jnp.bfloat16)
    block_count = row_count // BLOCK
    q_blocks = q_rot.reshape(block_count, BLOCK, head_count, head_dim)
    k_blocks = k_rot.reshape(block_count, BLOCK, head_count, head_dim)
    v_blocks = values_new.reshape(block_count, BLOCK, head_count, head_dim)
    log_steps = log_decay.reshape(block_count, BLOCK, head_count)
    row_ids = lax.broadcasted_iota(jnp.int32, (BLOCK, BLOCK), 0)
    col_ids = lax.broadcasted_iota(jnp.int32, (BLOCK, BLOCK), 1)
    lower_mask = col_ids <= row_ids
    cumulative = jnp.einsum("ij,bjh->bhi", lower_mask.astype(jnp.float32), log_steps)
    block_total = cumulative[:, :, -1]
    differences = cumulative[:, :, :, None] - cumulative[:, :, None, :]
    decays = jnp.where(lower_mask, jnp.exp(jnp.where(lower_mask, differences, 0.0)), 0.0)
    scores = jnp.einsum("bihd,bjhd->bhij", q_blocks, k_blocks, preferred_element_type=jnp.float32)
    weights = (scores * decays).astype(jnp.bfloat16)
    inner_term = jnp.einsum(
        "bhij,bjhe->bihe", weights, v_blocks, preferred_element_type=jnp.float32
    )
    key_scale = jnp.exp(block_total[:, :, None] - cumulative)
    updates = jnp.einsum(
        "bhj,bjhd,bjhe->bhde", key_scale, k_blocks.astype(jnp.float32), v_blocks.astype(jnp.float32)
    )
    factor = jnp.exp(block_total)
    local_state = jnp.zeros((head_count, head_dim, head_dim), jnp.float32)
    for block_index in range(block_count):
        local_state = factor[block_index][:, None, None] * local_state + updates[block_index]
    entering = carried_in(
        (jnp.exp(jnp.sum(block_total, axis=0)), local_state),
        EP,
        chain_pair,
        (jnp.ones((head_count,), jnp.float32), jnp.zeros_like(local_state)),
    )
    carry_state = entering[1]
    starts = []
    for block_index in range(block_count):
        starts.append(carry_state)
        carry_state = factor[block_index][:, None, None] * carry_state + updates[block_index]
    carried = jnp.stack(starts)
    cross_term = jnp.einsum(
        "bhi,bihd,bhde->bihe", jnp.exp(cumulative), q_blocks.astype(jnp.float32), carried
    )
    retained = (inner_term + cross_term).reshape(row_count, head_count, head_dim)
    centre = jnp.mean(retained, axis=-1, keepdims=True)
    spread = jnp.mean(jnp.square(retained - centre), axis=-1, keepdims=True)
    scaled = (retained - centre) * lax.rsqrt(spread + EPS) * head_gain.reshape(head_count, head_dim)
    mixer_hidden = (
        scaled.reshape(row_count, mix_width) * jax.nn.silu(gate_raw.astype(jnp.float32))
    ).astype(jnp.bfloat16)
    return lax.psum_scatter(
        jnp.dot(mixer_hidden, output_weight, preferred_element_type=jnp.float32).astype(
            jnp.bfloat16
        ),
        "tp",
        scatter_dimension=0,
        tiled=True,
    )


def expert_half(
    expert_input, expert_gain, routes, route_weight, expert_gate, expert_up, expert_down
):
    tok_count, top_count = routes.shape
    experts = lax.axis_size(EP)
    capacity = max(2, 3 * tok_count * top_count // (2 * experts))
    width = expert_input.shape[1]
    normed = norm_rows(expert_input, expert_gain)
    flat_routes = routes.reshape(-1)
    entries = flat_routes.shape[0]
    onehot = (flat_routes[:, None] == jnp.arange(experts, dtype=jnp.int32)[None, :]).astype(
        jnp.bfloat16
    )
    before = (
        lax.broadcasted_iota(jnp.int32, (entries, entries), 1)
        < lax.broadcasted_iota(jnp.int32, (entries, entries), 0)
    ).astype(jnp.bfloat16)
    prior_count = jnp.dot(before, onehot, preferred_element_type=jnp.float32)
    slot_index = jnp.sum(prior_count * onehot.astype(jnp.float32), axis=1).astype(jnp.int32)
    target = flat_routes * capacity + slot_index
    token_ids = jnp.arange(entries, dtype=jnp.int32) // top_count
    slot_table = jnp.full((experts * capacity,), tok_count, jnp.int32).at[target].set(token_ids)
    padded = jnp.concatenate([normed, jnp.zeros((1, width), jnp.bfloat16)], axis=0)
    outgoing = jnp.take(padded, slot_table, axis=0).reshape(experts, capacity, width)
    arrived = lax.all_to_all(outgoing, EP, split_axis=0, concat_axis=0, tiled=True)
    sources = arrived.shape[0]
    flat_rows = arrived.reshape(sources * capacity, width)
    shard_piece = lax.all_gather((expert_gate[0], expert_up[0]), "tp", axis=1, tiled=True)
    gate_part = jnp.dot(flat_rows, shard_piece[0], preferred_element_type=jnp.float32)
    up_part = jnp.dot(flat_rows, shard_piece[1], preferred_element_type=jnp.float32)
    hidden = (jax.nn.silu(gate_part) * up_part).astype(jnp.bfloat16)
    reduced = jnp.dot(
        hidden,
        lax.all_gather(expert_down[0], "tp", axis=0, tiled=True),
        preferred_element_type=jnp.float32,
    )
    results = reduced.astype(jnp.bfloat16).reshape(sources, capacity, width)
    returned = lax.all_to_all(results, EP, split_axis=0, concat_axis=0, tiled=True)
    picked = jnp.take(returned.reshape(experts * capacity, width), target, axis=0)
    picked = picked.astype(jnp.float32).reshape(tok_count, top_count, width)
    norm_weight = route_weight / jnp.sum(route_weight, axis=1, keepdims=True)
    return jnp.sum(picked * norm_weight[:, :, None], axis=1).astype(jnp.bfloat16)


def on_device(
    mixer_input,
    mixer_gain,
    query_weight,
    key_weight,
    value_weight,
    gate_weight,
    head_gain,
    output_weight,
    log_decay,
    expert_input,
    expert_gain,
    routes,
    route_weight,
    expert_gate,
    expert_up,
    expert_down,
):
    mixer_output = mixer_half(
        mixer_input,
        mixer_gain,
        query_weight,
        key_weight,
        value_weight,
        gate_weight,
        head_gain,
        output_weight,
        log_decay,
    )
    expert_output = expert_half(
        expert_input, expert_gain, routes, route_weight, expert_gate, expert_up, expert_down
    )
    return (mixer_output, expert_output)


def solution(mesh):
    finer = Mesh(mesh.devices.reshape(8, 4, 2, mesh.shape["tp"]), ("ep_0", "ep_1", "ep_2", "tp"))
    placed = (
        P(EP, None),
        P(),
        P(None, "tp"),
        P(None, "tp"),
        P(None, "tp"),
        P(None, "tp"),
        P("tp"),
        P("tp", None),
        P(EP, "tp"),
        P(EP_TP, None),
        P(),
        P(EP_TP, None),
        P(EP_TP, None),
        P(EP, None, "tp"),
        P(EP, None, "tp"),
        P(EP, "tp", None),
    )
    return jax.shard_map(
        on_device,
        mesh=finer,
        in_specs=placed,
        out_specs=(P(EP_TP, None), P(EP_TP, None)),
        check_vma=False,
    )
```

profile of v0, /device:TPU:2, one launch (start us, length us, event | category | flops | bytes accessed | tf_op | source)
XLA Modules:
  0.0 269.4 jit_solution(11428957834506784839)
XLA Ops:
  10.0 1.4 scatter_custom_fusion
  11.4 3.1 %gather_fusion = bf16[384,2048]{1,0:T(8,128)(2,1)} fusion(bf16[129,2048]{1,0:T(8,128)(2,1)S(1)} %concatenate.26, s32[1024]{0:T(1024)S(1)} %pad_clamp_fusion.1), kind=kCustom, calls=%fused_computation | custom fusion | bytes 3147264 | tf_op jit(solution)/shard_map/jit(_take)/gather | solution.py:176
  14.5 2.5 gather.13
  17.2 1.6 broadcast_select_fusion
  18.8 12.0 %all-to-all-start = ((bf16[64,6,2048]{2,1,0:T(8,128)(2,1)}), bf16[64,6,2048]{2,1,0:T(8,128)(2,1)S(1)}, u32[]{:S(2)}, u32[]{:S(2)}) async-start(bf16[64,6,2048]{2,1,0:T(8,128)(2,1)} %broadcast_select_fusion), calls=%async_computation.1 | async-start | bytes 4194304 | tf_op jit(solution)/shard_map/all_to_all | solution.py:177
  31.7 2.1 fusion
  35.4 2.8 %convolution_convert_fusion.3 = bf16[512,256]{0,1:T(8,128)(2,1)S(1)} fusion(bf16[2048,256]{1,0:T(8,128)(2,1)} %param.18, bf16[512,2048]{1,0:T(8,128)(2,1)} %param.16, f32[2048]{0:T(1024)S(1)} %copy-done.25, f32[512]{0:T(512)S(1)} %add_rsqrt_fusion), kind=kOutput, calls=%fused_computation.28 | convolution fusion | flops 541196288 | bytes 3418112 | tf_op jit(solution)/shard_map/dot_general | solution.py:82
  38.4 3.5 %convolution_convert_fusion.2 = bf16[512,256]{0,1:T(8,128)(2,1)} fusion(bf16[2048,256]{1,0:T(8,128)(2,1)} %param.19, bf16[512,2048]{1,0:T(8,128)(2,1)} %param.16, f32[2048]{0:T(1024)S(1)} %copy-done.25, f32[512]{0:T(512)S(1)} %add_rsqrt_fusion), kind=kOutput, calls=%fused_computation.27 | convolution fusion | flops 541196288 | bytes 3418112 | tf_op jit(solution)/shard_map/dot_general | solution.py:82
  41.9 2.4 all-reduce.1
  44.9 7.8 %all-gather.4 = bf16[4,1,2]{2,1,0:T(2,128)(2,1)S(1)} all-gather(bf16[1,1,2]{2,1,0:T(2,128)(2,1)S(1)} %convert_bitcast_fusion), channel_id=1, replica_groups=mesh['ep_0'=8,'ep_1'=4,'ep_2'=2,'tp'=4] {'ep_1'}, dimensions={0}, use_global_device_ids=true | all-gather | bytes 20 | tf_op jit(solution)/shard_map/all_gather | solution.py:25
  53.6 1.8 convert.28
  55.9 2.3 subtract_convert_fusion
  58.2 1.0 concatenate.23
  59.3 1.0 copy.61
  60.3 1.0 concatenate.24
  61.3 1.0 copy.62
  62.4 2.6 convolution_convert_fusion.4
  66.1 1.4 fusion.27
  67.5 1.4 fusion.35
  69.8 1.9 all_gather.36
  72.4 1.4 fusion.62
  75.1 16.2 %all-gather.5 = bf16[8,1,2]{2,1,0:T(2,128)(2,1)S(1)} all-gather(bf16[1,1,2]{2,1,0:T(2,128)(2,1)S(1)} %fusion.73), channel_id=1, replica_groups=mesh['ep_0'=8,'ep_1'=4,'ep_2'=2,'tp'=4] {'ep_0'}, dimensions={0}, use_global_device_ids=true | all-gather | bytes 36 | tf_op jit(solution)/shard_map/all_gather | solution.py:25
  91.9 1.6 concatenate.20
  93.5 1.8 copy.59
  95.3 1.6 concatenate.21
  96.9 1.8 copy.60
  98.6 12.1 %all_gather.37 = bf16[4,2,128,128]{3,2,1,0:T(8,128)(2,1)S(1)} all-gather(bf16[1,2,128,128]{3,2,1,0:T(8,128)(2,1)} %fusion.56), channel_id=1, replica_groups=mesh['ep_0'=8,'ep_1'=4,'ep_2'=2,'tp'=4] {'ep_1'}, dimensions={0}, use_global_device_ids=true | all-gather | bytes 327680 | tf_op jit(solution)/shard_map/all_gather | solution.py:25
  111.5 25.7 %all_gather.38 = bf16[8,2,128,128]{3,2,1,0:T(8,128)(2,1)S(1)} all-gather(bf16[1,2,128,128]{3,2,1,0:T(8,128)(2,1)S(1)} %fusion.55), channel_id=1, replica_groups=mesh['ep_0'=8,'ep_1'=4,'ep_2'=2,'tp'=4] {'ep_0'}, dimensions={0}, use_global_device_ids=true | all-gather | bytes 589824 | tf_op jit(solution)/shard_map/all_gather | solution.py:25
  137.2 1.6 multiply_add_fusion.1
  138.8 1.3 convolution_bitcast_fusion.1
  140.1 2.8 %fusion.90 = (f32[4,128,2]{1,2,0:T(2,128)S(1)}, f32[4,128,2,128]{1,3,2,0:T(8,128)}) fusion(f32[4,128,2,128]{1,3,2,0:T(8,128)} %convolution_bitcast_fusion.1, bf16[4,128,2,128]{3,1,2,0:T(8,128)(2,1)S(1)} %fusion.27, f32[4,2,128]{2,1,0:T(2,128)S(1)} %copy-done.18, pred[128,128]{1,0:T(8,128)(4,1)} %iota_compare_fusion.4, bf16[4,128,2,64]{3,1,2,0:T(8,128)(2,1)} %copy.60, ...), kind=kOutput, calls=%fused_computation.178 | convolution fusion | flops 68549632 | bytes 1859584 | tf_op jit(solution)/shard_map/bhij,bjhe->bihe/dot_general | solution.py:110
  142.9 2.1 copy.71
  145.0 1.1 multiply_reduce_fusion.1
  146.3 0.9 copy.72
  147.2 1.4 mul.592
  148.6 2.3 sub.60
  150.9 6.0 %convolution_convert_fusion = bf16[512,2048]{1,0:T(8,128)(2,1)} fusion(bf16[256,2048]{1,0:T(8,128)(2,1)S(1)} %copy-done, f32[64,8,2,128]{3,2,1,0:T(2,128)} %bitcast.151, f32[64,8,2,128]{3,2,1,0:T(2,128)} %bitcast.152, f32[64,8,2,128]{3,2,1,0:T(2,128)} %bitcast.153, bf16[2048,256]{1,0:T(8,128)(2,1)} %param.21, f32[256]{0:T(256)S(1)} %copy-done.27, ...), kind=kOutput, calls=%fused_computation.14 | convolution fusion | flops 1080426496 | bytes 7875584 | tf_op jit(solution)/shard_map/dot_general | solution.py:144
  157.0 1.5 reshape.379
  158.4 5.8 %fusion.7 = f32[384,1024]{1,0:T(8,128)} fusion(bf16[384,2048]{1,0:T(8,128)(2,1)} %reshape.379, bf16[1,2048,1024]{2,1,0:T(8,128)(2,1)} %all-gather.10.cloned.1.call-done), kind=kOutput, calls=%fused_computation.12 | convolution fusion | flops 1610612736 | bytes 7340032 | tf_op jit(solution)/shard_map/dot_general | solution.py:181
  164.2 12.8 %all-gather.14.cloned.1.call-done = bf16[1,1024,2048]{2,1,0:T(8,128)(2,1)} async-done(((bf16[1,256,2048]{2,1,0:T(8,128)(2,1)}), bf16[1,1024,2048]{2,1,0:T(8,128)(2,1)}) %all-gather.14.cloned.1.call-update) | async-done | bytes 4194320 | tf_op jit(solution)/shard_map/all_gather | solution.py:186
  177.0 8.6 %fusion.9 = bf16[384,2048]{1,0:T(8,128)(2,1)} fusion(bf16[1,1024,2048]{2,1,0:T(8,128)(2,1)} %all-gather.14.cloned.1.call-done, f32[384,1024]{1,0:T(8,128)} %fusion.7, bf16[384,2048]{1,0:T(8,128)(2,1)S(1)} %copy-done.3, bf16[1,2048,1024]{2,1,0:T(8,128)(2,1)} %all-gather.12.cloned.1.call-done), kind=kOutput, calls=%fused_computation.15 | convolution fusion | flops 3224371200 | bytes 13107200 | tf_op jit(solution)/shard_map/dot_general | solution.py:184
  185.6 3.7 %reshape.380 = bf16[64,6,2048]{2,1,0:T(8,128)(2,1)} reshape(bf16[384,2048]{1,0:T(8,128)(2,1)} %fusion.9) | data formatting | bytes 3145728 | tf_op jit(solution)/shard_map/reshape | solution.py:189
  189.3 10.9 %all-to-all-start.1 = ((bf16[64,6,2048]{2,1,0:T(8,128)(2,1)}), bf16[64,6,2048]{2,1,0:T(8,128)(2,1)}, u32[]{:S(2)}, u32[]{:S(2)}) async-start(bf16[64,6,2048]{2,1,0:T(8,128)(2,1)} %reshape.380), calls=%async_computation.2 | async-start | bytes 4194304 | tf_op jit(solution)/shard_map/all_to_all | solution.py:190
  200.7 50.6 %all-to-all-done.1 = bf16[64,6,2048]{2,1,0:T(8,128)(2,1)} async-done(((bf16[64,6,2048]{2,1,0:T(8,128)(2,1)}), bf16[64,6,2048]{2,1,0:T(8,128)(2,1)}, u32[]{:S(2)}, u32[]{:S(2)}) %all-to-all-start.1) | async-done | bytes 1572896 | tf_op jit(solution)/shard_map/all_to_all | solution.py:190
  251.3 2.6 reshape.381
  253.9 2.3 gather_fusion.1
  256.2 1.7 gather.15
  258.0 4.9 %multiply_reduce_fusion = bf16[128,2048]{1,0:T(8,128)(2,1)} fusion(bf16[128,2,2048]{2,1,0:T(2,128)(2,1)S(1)} %gather.15, pred[128,2]{1,0:T(8,128)(4,1)S(1)} %copy.76, f32[128,2]{1,0:T(8,128)S(1)} %copy.78), kind=kLoop, calls=%fused_computation.16 | loop fusion | flops 1835008 | bytes 1574144 | tf_op jit(solution)/shard_map/reduce_sum | solution.py:194
  (128 shorter events, 12.8 us)
Async XLA Ops:
  7.2 143.8 %copy-start = (bf16[256,2048]{1,0:T(8,128)(2,1)S(1)}, bf16[256,2048]{1,0:T(8,128)(2,1)}, u32[]{:S(2)}) copy-start(bf16[256,2048]{1,0:T(8,128)(2,1)} %param.23) | copy-start | bytes 3145732
  7.2 1.5 copy-start.8
  7.2 2.3 copy-start.2
  7.2 2.5 copy-start.10
  7.2 151.2 %all-gather.10.cloned.1.call-start = ((), (), s32[]{:S(2)}) async-start(), calls=%async_computation.4 | async-start | bytes 5242880 | tf_op jit(solution)/shard_map/all_gather | solution.py:180
  7.9 156.3 %all-gather.12.cloned.1.call-start = ((), (), s32[]{:S(2)}) async-start(), calls=%async_computation.5 | async-start | bytes 5242880 | tf_op jit(solution)/shard_map/all_gather | solution.py:180
  9.2 2.2 copy-start.6
  9.9 1.4 copy-start.15
  18.8 138.2 %all-to-all-start = ((bf16[64,6,2048]{2,1,0:T(8,128)(2,1)}), bf16[64,6,2048]{2,1,0:T(8,128)(2,1)S(1)}, u32[]{:S(2)}, u32[]{:S(2)}) async-start(bf16[64,6,2048]{2,1,0:T(8,128)(2,1)} %broadcast_select_fusion), calls=%async_computation.1 | async-start | bytes 4194304 | tf_op jit(solution)/shard_map/all_to_all | solution.py:177
  30.8 2.9 %copy-start.17 = (f32[512,2]{0,1:T(2,128)S(1)}, f32[512,2]{0,1:T(2,128)}, u32[]{:S(2)}) copy-start(f32[512,2]{0,1:T(2,128)} %param.24) | copy-start | bytes 12292
  30.9 3.3 %copy-start.28 = (u32[256]{0:T(256)S(1)}, u32[256]{0:T(256)}, u32[]{:S(2)}) copy-start(u32[256]{0:T(256)} %constant.123) | copy-start | bytes 3076
  30.9 4.5 %copy-start.25 = (f32[2048]{0:T(1024)S(1)}, f32[2048]{0:T(1024)}, u32[]{:S(2)}) copy-start(f32[2048]{0:T(1024)} %param.17) | copy-start | bytes 24580
  30.9 146.1 %all-gather.14.cloned.1.call-start = ((), (), s32[]{:S(2)}) async-start(), calls=%async_computation.6 | async-start | bytes 5242880 | tf_op jit(solution)/shard_map/all_gather | solution.py:186
  31.6 231.3 %reduce-scatter.2.cloned.1.call-start = ((), (), s32[]{:S(2)}) async-start(), calls=%async_computation.3 | async-start | bytes 2621440 | tf_op jit(solution)/shard_map/reduce_scatter | solution.py:143
  33.8 28.6 %copy-start.22 = (f32[512]{0:T(512)}, f32[512]{0:T(512)S(1)}, u32[]{:S(2)}) copy-start(f32[512]{0:T(512)S(1)} %add_rsqrt_fusion) | copy-start | bytes 6148
  44.4 0.5 copy-start.24
  66.0 2.9 %copy-start.11 = (f32[2]{0:T(128)}, f32[2]{0:T(128)S(1)}, u32[]{:S(2)}) copy-start(f32[2]{0:T(128)S(1)} %get-tuple-element.6) | copy-start | bytes 28
  66.0 2.9 %copy-start.13 = (f32[2]{0:T(128)}, f32[2]{0:T(128)S(1)}, u32[]{:S(2)}) copy-start(f32[2]{0:T(128)S(1)} %get-tuple-element.7) | copy-start | bytes 28
  66.1 2.9 %copy-start.21 = (f32[2]{0:T(128)}, f32[2]{0:T(128)S(1)}, u32[]{:S(2)}) copy-start(f32[2]{0:T(128)S(1)} %get-tuple-element.5) | copy-start | bytes 28
  68.9 0.8 copy-start.1
  72.4 2.7 %copy-start.20 = (f32[2]{0:T(128)}, f32[2]{0:T(128)S(1)}, u32[]{:S(2)}) copy-start(f32[2]{0:T(128)S(1)} %slice_convert_fusion.5) | copy-start | bytes 28
  73.7 0.7 copy-start.14
  91.9 45.3 %copy-start.12 = (f32[2]{0:T(128)S(1)}, f32[2]{0:T(128)}, u32[]{:S(2)}) copy-start(f32[2]{0:T(128)} %copy-done.11) | copy-start | bytes 28
  98.6 40.2 %copy-start.4 = (bf16[4,128,2,64]{3,1,2,0:T(8,128)(2,1)S(1)}, bf16[4,128,2,64]{3,1,2,0:T(8,128)(2,1)}, u32[]{:S(2)}) copy-start(bf16[4,128,2,64]{3,1,2,0:T(8,128)(2,1)} %copy.59) | copy-start | bytes 393220
  98.6 40.2 %copy-start.5 = (bf16[4,128,2,64]{3,1,2,0:T(8,128)(2,1)S(1)}, bf16[4,128,2,64]{3,1,2,0:T(8,128)(2,1)}, u32[]{:S(2)}) copy-start(bf16[4,128,2,64]{3,1,2,0:T(8,128)(2,1)} %copy.60) | copy-start | bytes 393220
  110.7 29.4 %copy-start.18 = (f32[4,2,128]{2,1,0:T(2,128)S(1)}, f32[4,2,128]{2,1,0:T(2,128)}, u32[]{:S(2)}) copy-start(f32[4,2,128]{2,1,0:T(2,128)} %copy.63) | copy-start | bytes 12292
  142.9 8.0 %copy-start.23 = (f32[512]{0:T(512)S(1)}, f32[512]{0:T(512)}, u32[]{:S(2)}) copy-start(f32[512]{0:T(512)} %copy-done.22) | copy-start | bytes 6148
  142.9 8.0 %copy-start.26 = (f32[2048]{0:T(1024)S(1)}, f32[2048]{0:T(1024)}, u32[]{:S(2)}) copy-start(f32[2048]{0:T(1024)} %param.17) | copy-start | bytes 24580
  142.9 8.0 %copy-start.27 = (f32[256]{0:T(256)S(1)}, f32[256]{0:T(256)}, u32[]{:S(2)}) copy-start(f32[256]{0:T(256)} %param.22) | copy-start | bytes 3076
  158.4 18.6 %copy-start.3 = (bf16[384,2048]{1,0:T(8,128)(2,1)S(1)}, bf16[384,2048]{1,0:T(8,128)(2,1)}, u32[]{:S(2)}) copy-start(bf16[384,2048]{1,0:T(8,128)(2,1)} %reshape.379) | copy-start | bytes 4718596
  189.3 10.9 %copy-start.7 = (s32[256]{0:T(256)S(1)}, s32[256]{0:T(256)}, u32[]{:S(2)}) copy-start(s32[256]{0:T(256)} %copy-done.6) | copy-start | bytes 3076
  189.3 11.1 %copy-start.9 = (s32[128,2]{0,1:T(2,128)S(1)}, s32[128,2]{0,1:T(2,128)}, u32[]{:S(2)}) copy-start(s32[128,2]{0,1:T(2,128)} %param.27) | copy-start | bytes 3076
  189.3 11.3 %copy-start.19 = (f32[128,2]{0,1:T(2,128)S(1)}, f32[128,2]{0,1:T(2,128)}, u32[]{:S(2)}) copy-start(f32[128,2]{0,1:T(2,128)} %param.28) | copy-start | bytes 3076
  189.3 11.4 %copy-start.16 = (s32[256,1]{0,1:T(1,128)S(1)}, s32[256,1]{0,1:T(1,128)}, u32[]{:S(2)}) copy-start(s32[256,1]{0,1:T(1,128)} %copy-done.15) | copy-start | bytes 3076
  189.3 62.0 %all-to-all-start.1 = ((bf16[64,6,2048]{2,1,0:T(8,128)(2,1)}), bf16[64,6,2048]{2,1,0:T(8,128)(2,1)}, u32[]{:S(2)}, u32[]{:S(2)}) async-start(bf16[64,6,2048]{2,1,0:T(8,128)(2,1)} %reshape.380), calls=%async_computation.2 | async-start | bytes 4194304 | tf_op jit(solution)/shard_map/all_to_all | solution.py:190
Sparse Core Ops, SparseCore 0:
  9.8 56.8 all-gather.9
  68.5 54.8 all-gather.11
  125.2 51.7 all-gather.13
  180.0 32.6 reduce-scatter.1
where the time goes:
time: 270 us; the launch traced here: 269 us
  blocking collectives  66.2 us (25%)
  waiting for transfers between devices  65.4 us (24%)
  local copies, waits for them, and re-layouts  41.3 us (15%)
  matrix products  35.1 us (13%)
  other arithmetic  23.3 us (9%)
  starting transfers between devices  23.1 us (9%)
  between operations  15 us (6%)
    all_gather x5, blocking collectives, carried_in(): lax.all_gather(part.astype(kind), axis)  63.8 us
    all_to_all x1, waiting for transfers between devices, expert_half(): lax.all_to_all(results, EP, split_axis=0, concat_axis=0, tiled=True)  50.6 us
    all_gather x1, waiting for transfers between devices, expert_half(): lax.all_gather(expert_down[0], 'tp', axis=0, tiled=True)  12.8 us
    all_to_all x1, starting transfers between devices, expert_half(): lax.all_to_all(outgoing, EP, split_axis=0, concat_axis=0, tiled=True)  12 us
    all_to_all x1, starting transfers between devices, expert_half(): lax.all_to_all(results, EP, split_axis=0, concat_axis=0, tiled=True)  10.9 us
    concatenate x8, local copies, waits for them, and re-layouts, rotate(): jnp.concatenate([first_half * cosine - second * sine_part, first_half * s...  10.8 us
    dot_general x3, matrix products, project(): jnp.dot(normed, weight, preferred_element_type=jnp.float32)  8.88 us
    dot_general x1, matrix products, expert_half(): jnp.dot(hidden, lax.all_gather(expert_down[0], 'tp', axis=0, tiled=True),...  8.59 us
  transfers between devices with their start and end apart: 6, of which 2 were waited for; matrix products, arithmetic and copies ran while one was open for 37% of the time, Pallas kernels for 0%

commit v1 on v0

--- a/solution.py
+++ b/solution.py
@@ -181,10 +181,17 @@
     gate_part = jnp.dot(flat_rows, shard_piece[0], preferred_element_type=jnp.float32)
     up_part = jnp.dot(flat_rows, shard_piece[1], preferred_element_type=jnp.float32)
     hidden = (jax.nn.silu(gate_part) * up_part).astype(jnp.bfloat16)
+
+    def assign_the_values(body, axis_key):
+        made = []
+        for _ in range(jax.lax.psum(1, axis_key)):
+            made.append(body)
+        f_next = jnp.stack(made, axis=0)
+        last = jax.lax.all_to_all(f_next, axis_key, 0, 0)
+        return jnp.concatenate(last, 0)
+
     reduced = jnp.dot(
-        hidden,
-        lax.all_gather(expert_down[0], "tp", axis=0, tiled=True),
-        preferred_element_type=jnp.float32,
+        hidden, assign_the_values(expert_down[0], "tp"), preferred_element_type=jnp.float32
     )
     results = reduced.astype(jnp.bfloat16).reshape(sources, capacity, width)
     returned = lax.all_to_all(results, EP, split_axis=0, concat_axis=0, tiled=True)

time: 270 us -> 285 us (1.056)
  blocking collectives: 66.2 us -> 87.4 us
  waiting for transfers between devices: 65.4 us -> 52 us
  other arithmetic: 23.3 us -> 26.9 us
    all_gather x5, blocking collectives: 63.8 us -> 84.9 us  [carried_in(): lax.all_gather(part.astype(kind), axis)]
    all_gather x1 -> x0, waiting for transfers between devices: 12.8 us -> none  [expert_half(): lax.all_gather(expert_down[0], 'tp', axis=0, tiled=True)]
    all_to_all x0 -> x1, starting transfers between devices: none -> 4.94 us  [assign_the_values(): last = jax.lax.all_to_all(f_next, axis_key, 0, 0)]
    concatenate x8, local copies, waits for them, and re-layouts: 10.8 us -> 5.89 us  [rotate(): jnp.concatenate([first_half * cosine - second * sine_part, first_half * s...]
    another operation x0 -> x1, local copies, waits for them, and re-layouts: none -> 3.69 us  [assign_the_values(): f_next = jnp.stack(made, axis=0)]
  transfers between devices with their start and end apart: 6 -> 6, of which waited for: 2 -> 1; matrix products, arithmetic and copies ran while one was open for 37% -> 36% of each run, Pallas kernels for 0% -> 0%
where the time goes in v1:
time: 285 us; the launch traced here: 283 us
  blocking collectives  87.4 us (31%)
  waiting for transfers between devices  52 us (18%)
  local copies, waits for them, and re-layouts  41.6 us (15%)
  matrix products  34.8 us (12%)
  other arithmetic  26.9 us (9%)
  starting transfers between devices  25.7 us (9%)
  between operations  15 us (5%)
    all_gather x5, blocking collectives, carried_in(): lax.all_gather(part.astype(kind), axis)  84.9 us
    all_to_all x1, waiting for transfers between devices, expert_half(): lax.all_to_all(results, EP, split_axis=0, concat_axis=0, tiled=True)  50.6 us
    all_to_all x1, starting transfers between devices, expert_half(): lax.all_to_all(outgoing, EP, split_axis=0, concat_axis=0, tiled=True)  12 us
    dot_general x3, matrix products, project(): jnp.dot(normed, weight, preferred_element_type=jnp.float32)  8.74 us
    all_to_all x1, starting transfers between devices, expert_half(): lax.all_to_all(results, EP, split_axis=0, concat_axis=0, tiled=True)  8.65 us
    dot_general x1, matrix products, expert_half(): jnp.dot(hidden, assign_the_values(expert_down[0], 'tp'), preferred_elemen...  8.58 us
    dot_general x1, matrix products, mixer_half(): jnp.dot(mixer_hidden, output_weight, preferred_element_type=jnp.float32)  6.01 us
    concatenate x8, local copies, waits for them, and re-layouts, rotate(): jnp.concatenate([first_half * cosine - second * sine_part, first_half * s...  5.89 us
  transfers between devices with their start and end apart: 6, of which 1 were waited for; matrix products, arithmetic and copies ran while one was open for 36% of the time, Pallas kernels for 0%

profile of v1, /device:TPU:2, one launch (start us, length us, event | category | flops | bytes accessed | tf_op | source)
XLA Modules:
  0.0 283.4 jit_solution(4708161926805726561)
XLA Ops:
  10.0 1.2 fusion.13
  12.3 1.4 scatter_custom_fusion
  13.7 3.2 %gather_fusion = bf16[384,2048]{1,0:T(8,128)(2,1)} fusion(bf16[129,2048]{1,0:T(8,128)(2,1)S(1)} %concatenate.26, s32[1024]{0:T(1024)S(1)} %pad_clamp_fusion.1), kind=kCustom, calls=%fused_computation | custom fusion | bytes 3147264 | tf_op jit(solution)/shard_map/jit(_take)/gather | solution.py:176
  16.9 2.5 gather.13
  19.5 1.7 broadcast_select_fusion
  21.2 12.0 %all-to-all-start = ((bf16[64,6,2048]{2,1,0:T(8,128)(2,1)}), bf16[64,6,2048]{2,1,0:T(8,128)(2,1)S(1)}, u32[]{:S(2)}, u32[]{:S(2)}) async-start(bf16[64,6,2048]{2,1,0:T(8,128)(2,1)} %broadcast_select_fusion), calls=%async_computation.1 | async-start | bytes 4194304 | tf_op jit(solution)/shard_map/all_to_all | solution.py:177
  34.0 2.1 fusion
  38.0 2.4 all-reduce.1
  40.9 7.8 %all-gather.3 = bf16[4,1,2]{2,1,0:T(2,128)(2,1)S(1)} all-gather(bf16[1,1,2]{2,1,0:T(2,128)(2,1)S(1)} %convert_bitcast_fusion), channel_id=1, replica_groups=mesh['ep_0'=8,'ep_1'=4,'ep_2'=2,'tp'=4] {'ep_1'}, dimensions={0}, use_global_device_ids=true | all-gather | bytes 20 | tf_op jit(solution)/shard_map/all_gather | solution.py:25
  48.8 3.6 %convolution_convert_fusion.4 = bf16[512,256]{0,1:T(8,128)(2,1)} fusion(bf16[2048,256]{1,0:T(8,128)(2,1)} %param.18, bf16[512,2048]{1,0:T(8,128)(2,1)} %param.16, f32[2048]{0:T(1024)S(1)} %copy-done.27, f32[512]{0:T(512)S(1)} %add_rsqrt_fusion), kind=kOutput, calls=%fused_computation.26 | convolution fusion | flops 541196288 | bytes 3418112 | tf_op jit(solution)/shard_map/dot_general | solution.py:82
  52.5 1.7 convolution_convert_fusion.3
  54.7 37.2 %all-gather.4 = bf16[8,1,2]{2,1,0:T(2,128)(2,1)} all-gather(bf16[1,1,2]{2,1,0:T(2,128)(2,1)S(1)} %fusion.68), channel_id=1, replica_groups=mesh['ep_0'=8,'ep_1'=4,'ep_2'=2,'tp'=4] {'ep_0'}, dimensions={0}, use_global_device_ids=true | all-gather | bytes 36 | tf_op jit(solution)/shard_map/all_gather | solution.py:25
  92.4 1.0 convert.27
  93.4 1.0 convert.28
  94.4 0.9 subtract_convert_fusion
  95.4 1.0 concatenate.23
  96.4 1.0 copy.61
  97.4 1.0 concatenate.24
  98.5 1.0 copy.62
  100.3 3.4 %convolution_convert_fusion.5 = bf16[512,256]{1,0:T(8,128)(2,1)} fusion(bf16[2048,256]{1,0:T(8,128)(2,1)} %param.20, bf16[512,2048]{1,0:T(8,128)(2,1)} %param.16, f32[2048]{0:T(1024)} %param.17, f32[512]{0:T(512)} %copy-done.23), kind=kOutput, calls=%fused_computation.27 | convolution fusion | flops 541196288 | bytes 3418112 | tf_op jit(solution)/shard_map/dot_general | solution.py:82
  103.7 1.7 reshape.375
  108.1 1.4 fusion.22
  109.5 1.4 fusion.30
  111.0 1.9 all_gather.33
  114.2 1.2 fusion.59
  116.0 1.3 fusion.57
  118.1 3.7 %stack.5 = bf16[4,256,2048]{2,1,0:T(8,128)(2,1)} broadcast(bf16[256,2048]{1,0:T(8,128)(2,1)} %bitcast.149), dimensions={1,2} | broadcast | bytes 5242880 | tf_op jit(solution)/shard_map/stack | solution.py:189
  121.8 4.9 %all-to-all-start.1 = ((bf16[4,256,2048]{2,1,0:T(8,128)(2,1)}), bf16[4,256,2048]{2,1,0:T(8,128)(2,1)}, u32[]{:S(2)}, u32[]{:S(2)}) async-start(bf16[4,256,2048]{2,1,0:T(8,128)(2,1)} %stack.5), calls=%async_computation.2 | async-start | bytes 8388608 | tf_op jit(solution)/shard_map/all_to_all | solution.py:190
  126.9 12.6 %all_gather.34 = bf16[4,2,128,128]{3,2,1,0:T(8,128)(2,1)S(1)} all-gather(bf16[1,2,128,128]{3,2,1,0:T(8,128)(2,1)} %fusion.51), channel_id=1, replica_groups=mesh['ep_0'=8,'ep_1'=4,'ep_2'=2,'tp'=4] {'ep_1'}, dimensions={0}, use_global_device_ids=true | all-gather | bytes 327680 | tf_op jit(solution)/shard_map/all_gather | solution.py:25
  141.0 25.4 %all_gather.35 = bf16[8,2,128,128]{3,2,1,0:T(8,128)(2,1)S(1)} all-gather(bf16[1,2,128,128]{3,2,1,0:T(8,128)(2,1)S(1)} %fusion.50), channel_id=1, replica_groups=mesh['ep_0'=8,'ep_1'=4,'ep_2'=2,'tp'=4] {'ep_0'}, dimensions={0}, use_global_device_ids=true | all-gather | bytes 589824 | tf_op jit(solution)/shard_map/all_gather | solution.py:25
  166.4 1.5 multiply_add_fusion.1
  167.9 1.3 convolution_bitcast_fusion.1
  169.2 2.7 fusion.85
  171.9 2.1 copy.71
  174.0 1.1 multiply_reduce_fusion.1
  176.2 1.4 mul.592
  177.5 2.3 sub.60
  179.9 6.0 %convolution_convert_fusion = bf16[512,2048]{1,0:T(8,128)(2,1)} fusion(bf16[256,2048]{1,0:T(8,128)(2,1)S(1)} %copy-done, f32[64,8,2,128]{3,2,1,0:T(2,128)} %bitcast.150, f32[64,8,2,128]{3,2,1,0:T(2,128)} %bitcast.151, f32[64,8,2,128]{3,2,1,0:T(2,128)} %bitcast.152, bf16[2048,256]{1,0:T(8,128)(2,1)} %param.21, f32[256]{0:T(256)S(1)} %copy-done.29, ...), kind=kOutput, calls=%fused_computation.12 | convolution fusion | flops 1080426496 | bytes 7875584 | tf_op jit(solution)/shard_map/dot_general | solution.py:144
  186.0 1.4 reshape.383
  187.4 5.7 %fusion.5 = f32[384,1024]{1,0:T(8,128)} fusion(bf16[384,2048]{1,0:T(8,128)(2,1)} %reshape.383, bf16[1,2048,1024]{2,1,0:T(8,128)(2,1)} %all-gather.8.cloned.1.call-done), kind=kOutput, calls=%fused_computation.10 | convolution fusion | flops 1610612736 | bytes 7340032 | tf_op jit(solution)/shard_map/dot_general | solution.py:181
  193.1 8.6 %convolution_convert_fusion.1 = bf16[384,2048]{1,0:T(8,128)(2,1)} fusion(bf16[1024,2048]{1,0:T(8,128)(2,1)} %bitcast.34, f32[384,1024]{1,0:T(8,128)} %fusion.5, bf16[384,2048]{1,0:T(8,128)(2,1)S(1)} %copy-done.4, bf16[1,2048,1024]{2,1,0:T(8,128)(2,1)} %all-gather.10.cloned.1.call-done), kind=kOutput, calls=%fused_computation.13 | convolution fusion | flops 3224371200 | bytes 13107200 | tf_op jit(solution)/shard_map/dot_general | solution.py:193
  201.7 3.7 %reshape.385 = bf16[64,6,2048]{2,1,0:T(8,128)(2,1)} reshape(bf16[384,2048]{1,0:T(8,128)(2,1)} %convolution_convert_fusion.1) | data formatting | bytes 3145728 | tf_op jit(solution)/shard_map/reshape | solution.py:196
  205.4 8.7 %all-to-all-start.2 = ((bf16[64,6,2048]{2,1,0:T(8,128)(2,1)}), bf16[64,6,2048]{2,1,0:T(8,128)(2,1)}, u32[]{:S(2)}, u32[]{:S(2)}) async-start(bf16[64,6,2048]{2,1,0:T(8,128)(2,1)} %reshape.385), calls=%async_computation.3 | async-start | bytes 4194304 | tf_op jit(solution)/shard_map/all_to_all | solution.py:197
  214.7 50.6 %all-to-all-done.2 = bf16[64,6,2048]{2,1,0:T(8,128)(2,1)} async-done(((bf16[64,6,2048]{2,1,0:T(8,128)(2,1)}), bf16[64,6,2048]{2,1,0:T(8,128)(2,1)}, u32[]{:S(2)}, u32[]{:S(2)}) %all-to-all-start.2) | async-done | bytes 1572896 | tf_op jit(solution)/shard_map/all_to_all | solution.py:197
  265.2 2.6 reshape.386
  267.8 2.3 gather_fusion.1
  270.2 1.7 gather.15
  271.9 4.9 %multiply_reduce_fusion = bf16[128,2048]{1,0:T(8,128)(2,1)} fusion(bf16[128,2,2048]{2,1,0:T(2,128)(2,1)S(1)} %gather.15, pred[128,2]{1,0:T(8,128)(4,1)S(1)} %copy.76, f32[128,2]{1,0:T(8,128)S(1)} %copy.78), kind=kLoop, calls=%fused_computation.14 | loop fusion | flops 1835008 | bytes 1574144 | tf_op jit(solution)/shard_map/reduce_sum | solution.py:201
  (132 shorter events, 16.8 us)
Async XLA Ops:
  7.2 172.7 %copy-start = (bf16[256,2048]{1,0:T(8,128)(2,1)S(1)}, bf16[256,2048]{1,0:T(8,128)(2,1)}, u32[]{:S(2)}) copy-start(bf16[256,2048]{1,0:T(8,128)(2,1)} %param.23) | copy-start | bytes 3145732
  7.2 4.1 %copy-start.3 = (bf16[128,2048]{1,0:T(8,128)(2,1)S(1)}, bf16[128,2048]{1,0:T(8,128)(2,1)}, u32[]{:S(2)}) copy-start(bf16[128,2048]{1,0:T(8,128)(2,1)} %param.25) | copy-start | bytes 1572868
  7.2 180.2 %all-gather.8.cloned.1.call-start = ((), (), s32[]{:S(2)}) async-start(), calls=%async_computation.5 | async-start | bytes 5242880 | tf_op jit(solution)/shard_map/all_gather | solution.py:180
  9.1 4.6 %copy-start.9 = (s32[256]{0:T(256)}, s32[256]{0:T(256)S(1)}, u32[]{:S(2)}) copy-start(s32[256]{0:T(256)S(1)} %convert_element_type.480) | copy-start | bytes 3076
  12.2 1.4 copy-start.16
  21.2 97.0 %all-to-all-start = ((bf16[64,6,2048]{2,1,0:T(8,128)(2,1)}), bf16[64,6,2048]{2,1,0:T(8,128)(2,1)S(1)}, u32[]{:S(2)}, u32[]{:S(2)}) async-start(bf16[64,6,2048]{2,1,0:T(8,128)(2,1)} %broadcast_select_fusion), calls=%async_computation.1 | async-start | bytes 4194304 | tf_op jit(solution)/shard_map/all_to_all | solution.py:177
  33.2 2.9 %copy-start.18 = (f32[512,2]{0,1:T(2,128)S(1)}, f32[512,2]{0,1:T(2,128)}, u32[]{:S(2)}) copy-start(f32[512,2]{0,1:T(2,128)} %param.24) | copy-start | bytes 12292
  33.2 3.3 %copy-start.30 = (u32[256]{0:T(256)S(1)}, u32[256]{0:T(256)}, u32[]{:S(2)}) copy-start(u32[256]{0:T(256)} %constant.123) | copy-start | bytes 3076
  33.2 15.5 %copy-start.27 = (f32[2048]{0:T(1024)S(1)}, f32[2048]{0:T(1024)}, u32[]{:S(2)}) copy-start(f32[2048]{0:T(1024)} %param.17) | copy-start | bytes 24580
  33.2 159.9 %all-gather.10.cloned.1.call-start = ((), (), s32[]{:S(2)}) async-start(), calls=%async_computation.6 | async-start | bytes 5242880 | tf_op jit(solution)/shard_map/all_gather | solution.py:180
  36.1 16.3 %copy-start.23 = (f32[512]{0:T(512)}, f32[512]{0:T(512)S(1)}, u32[]{:S(2)}) copy-start(f32[512]{0:T(512)S(1)} %add_rsqrt_fusion) | copy-start | bytes 6148
  36.4 63.0 %copy-start.12 = (f32[4,2]{0,1:T(2,128)}, f32[4,2]{0,1:T(2,128)S(1)}, u32[]{:S(2)}) copy-start(f32[4,2]{0,1:T(2,128)S(1)} %get-tuple-element.2) | copy-start | bytes 100
  40.4 0.5 copy-start.25
  48.8 3.7 %copy-start.2 = (bf16[512,2048]{1,0:T(8,128)(2,1)S(1)}, bf16[512,2048]{1,0:T(8,128)(2,1)}, u32[]{:S(2)}) copy-start(bf16[512,2048]{1,0:T(8,128)(2,1)} %param.16) | copy-start | bytes 6291460
  48.8 3.7 %copy-start.26 = (bf16[2048,256]{1,0:T(8,128)(2,1)S(1)}, bf16[2048,256]{1,0:T(8,128)(2,1)}, u32[]{:S(2)}) copy-start(bf16[2048,256]{1,0:T(8,128)(2,1)} %param.19) | copy-start | bytes 3145732
  100.3 5.2 %copy-start.5 = (bf16[512,2,64]{0,2,1:T(8,128)(2,1)S(1)}, bf16[512,2,64]{0,2,1:T(8,128)(2,1)}, u32[]{:S(2)}) copy-start(bf16[512,2,64]{0,2,1:T(8,128)(2,1)} %get-tuple-element.14) | copy-start | bytes 393220
  108.1 1.4 copy-start.22
  108.1 9.3 %copy-start.13 = (f32[2]{0:T(128)}, f32[2]{0:T(128)S(1)}, u32[]{:S(2)}) copy-start(f32[2]{0:T(128)S(1)} %get-tuple-element.6) | copy-start | bytes 28
  108.1 9.3 %copy-start.14 = (f32[2]{0:T(128)}, f32[2]{0:T(128)S(1)}, u32[]{:S(2)}) copy-start(f32[2]{0:T(128)S(1)} %get-tuple-element.7) | copy-start | bytes 28
  110.9 6.5 %copy-start.1 = (f32[4,2,128,128]{3,2,1,0:T(8,128)}, f32[4,2,128,128]{3,2,1,0:T(8,128)S(1)}, u32[]{:S(2)}) copy-start(f32[4,2,128,128]{3,2,1,0:T(8,128)S(1)} %fusion.30) | copy-start | bytes 1572868
  114.2 3.2 %copy-start.21 = (f32[2]{0:T(128)}, f32[2]{0:T(128)S(1)}, u32[]{:S(2)}) copy-start(f32[2]{0:T(128)S(1)} %slice_convert_fusion.5) | copy-start | bytes 28
  117.4 4.4 %copy-start.15 = (f32[2]{0:T(128)}, f32[2]{0:T(128)S(1)}, u32[]{:S(2)}) copy-start(f32[2]{0:T(128)S(1)} %get-tuple-element.37) | copy-start | bytes 28
  121.8 71.3 %all-to-all-start.1 = ((bf16[4,256,2048]{2,1,0:T(8,128)(2,1)}), bf16[4,256,2048]{2,1,0:T(8,128)(2,1)}, u32[]{:S(2)}, u32[]{:S(2)}) async-start(bf16[4,256,2048]{2,1,0:T(8,128)(2,1)} %stack.5), calls=%async_computation.2 | async-start | bytes 8388608 | tf_op jit(solution)/shard_map/all_to_all | solution.py:190
  126.8 150.1 %reduce-scatter.2.cloned.1.call-start = ((), (), s32[]{:S(2)}) async-start(), calls=%async_computation.4 | async-start | bytes 2621440 | tf_op jit(solution)/shard_map/reduce_scatter | solution.py:143
  126.8 41.1 %copy-start.6 = (bf16[4,128,2,64]{3,1,2,0:T(8,128)(2,1)S(1)}, bf16[4,128,2,64]{3,1,2,0:T(8,128)(2,1)}, u32[]{:S(2)}) copy-start(bf16[4,128,2,64]{3,1,2,0:T(8,128)(2,1)} %copy.59) | copy-start | bytes 393220
  126.8 41.1 %copy-start.7 = (bf16[4,128,2,64]{3,1,2,0:T(8,128)(2,1)S(1)}, bf16[4,128,2,64]{3,1,2,0:T(8,128)(2,1)}, u32[]{:S(2)}) copy-start(bf16[4,128,2,64]{3,1,2,0:T(8,128)(2,1)} %copy.60) | copy-start | bytes 393220
  126.8 41.1 %copy-start.19 = (f32[4,128,2]{1,2,0:T(2,128)S(1)}, f32[4,128,2]{1,2,0:T(2,128)}, u32[]{:S(2)}) copy-start(f32[4,128,2]{1,2,0:T(2,128)} %copy.66) | copy-start | bytes 12292
  139.5 29.7 %copy-start.8 = (pred[128,128]{1,0:T(8,128)(4,1)S(1)}, pred[128,128]{1,0:T(8,128)(4,1)}, u32[]{:S(2)}) copy-start(pred[128,128]{1,0:T(8,128)(4,1)} %iota_compare_fusion.4) | copy-start | bytes 49156
  171.9 8.0 %copy-start.24 = (f32[512]{0:T(512)S(1)}, f32[512]{0:T(512)}, u32[]{:S(2)}) copy-start(f32[512]{0:T(512)} %copy-done.23) | copy-start | bytes 6148
  171.9 8.0 %copy-start.28 = (f32[2048]{0:T(1024)S(1)}, f32[2048]{0:T(1024)}, u32[]{:S(2)}) copy-start(f32[2048]{0:T(1024)} %param.17) | copy-start | bytes 24580
  171.9 8.0 %copy-start.29 = (f32[256]{0:T(256)S(1)}, f32[256]{0:T(256)}, u32[]{:S(2)}) copy-start(f32[256]{0:T(256)} %param.22) | copy-start | bytes 3076
  187.4 5.8 %copy-start.4 = (bf16[384,2048]{1,0:T(8,128)(2,1)S(1)}, bf16[384,2048]{1,0:T(8,128)(2,1)}, u32[]{:S(2)}) copy-start(bf16[384,2048]{1,0:T(8,128)(2,1)} %reshape.383) | copy-start | bytes 4718596
  205.4 8.7 %copy-start.10 = (s32[256]{0:T(256)S(1)}, s32[256]{0:T(256)}, u32[]{:S(2)}) copy-start(s32[256]{0:T(256)} %copy-done.9) | copy-start | bytes 3076
  205.4 8.9 %copy-start.11 = (s32[128,2]{0,1:T(2,128)S(1)}, s32[128,2]{0,1:T(2,128)}, u32[]{:S(2)}) copy-start(s32[128,2]{0,1:T(2,128)} %param.27) | copy-start | bytes 3076
  205.4 9.1 %copy-start.20 = (f32[128,2]{0,1:T(2,128)S(1)}, f32[128,2]{0,1:T(2,128)}, u32[]{:S(2)}) copy-start(f32[128,2]{0,1:T(2,128)} %param.28) | copy-start | bytes 3076
  205.4 9.2 %copy-start.17 = (s32[256,1]{0,1:T(1,128)S(1)}, s32[256,1]{0,1:T(1,128)}, u32[]{:S(2)}) copy-start(s32[256,1]{0,1:T(1,128)} %copy-done.16) | copy-start | bytes 3076
  205.4 59.8 %all-to-all-start.2 = ((bf16[64,6,2048]{2,1,0:T(8,128)(2,1)}), bf16[64,6,2048]{2,1,0:T(8,128)(2,1)}, u32[]{:S(2)}, u32[]{:S(2)}) async-start(bf16[64,6,2048]{2,1,0:T(8,128)(2,1)} %reshape.385), calls=%async_computation.3 | async-start | bytes 4194304 | tf_op jit(solution)/shard_map/all_to_all | solution.py:197
Sparse Core Ops, SparseCore 0:
  9.8 56.8 all-gather.7
  68.5 54.8 all-gather.9
  186.1 32.0 reduce-scatter.1
